TPU v7x, 32 devices: a whole 2x2x4 slice. The times are simulated.
32 devices in a mesh: sp: 16 (over z, y, core), tp: 2 (over x).
Axes of the slice: x: 2, y: 2, z: 4, core: 2. Of those that a mesh axis runs over, the one named last changes fastest.
Arguments:
- tokens: bfloat16 [1, 8192, 2048], P(None, ('sp', 'tp')), may hold values from -6 to 6
- input_norm_gain: float32 [2048], replicated, may hold values from 0.1 to 1.9
- query_weight: bfloat16 [2048, 1024], P(None, 'tp'), may hold values from -0.125 to 0.125
- forget_weight: bfloat16 [2048, 1024], P(None, 'tp'), may hold values from -0.125 to 0.125
- input_weight: bfloat16 [2048, 1024], P(None, 'tp'), may hold values from -0.125 to 0.125
- gate_weight: bfloat16 [2048, 1024], P(None, 'tp'), may hold values from -0.125 to 0.125
- slack: float32 [1024], P('tp'), may hold values from 0 to 0.06
- sudden_decay: float32 [1, 8192, 8], P(None, 'sp', 'tp'), may hold values from -0.75 to 0
- head_norm_gain: float32 [128], replicated, may hold values from 0.1 to 1.9
- output_weight: bfloat16 [1024, 2048], P(None, 'tp'), may hold values from -1.25 to 1.25
- output_norm_gain: float32 [2048], P('tp'), may hold values from 0.1 to 1.9
Outputs:
- mixer_output: bfloat16 [1, 8192, 2048], P(None, 'sp', 'tp')
All inputs are finite; a program needn't handle non-finite values.
Results may differ from a plain program's by a relative error of at most 0.0094.
Values may be sent and summed in bfloat16 or wider, within the bound.
A program may use at most 64 MiB of HBM per device.

v0:
```python
import jax
import jax.numpy as jnp
from jax import lax
from jax.sharding import PartitionSpec as P

D = 2048
KEY = 128
BLOCK = 64
epsilon = 1e-06
precise = lax.Precision.HIGHEST


def entering(part, axis, combine, identity):
    place = lax.axis_index(axis)
    gathered = jax.tree.map(lambda a: lax.all_gather(a, axis), part)
    state = jax.tree.map(lambda a, e: jnp.zeros_like(a) + jnp.asarray(e, a.dtype), part, identity)

    def one(turn, state):
        return combine(
            state, jax.tree.map(lambda a: lax.dynamic_index_in_dim(a, turn, 0, False), gathered)
        )

    return lax.fori_loop(0, place, one, state)


def normalize(tensor_in, gain_vec):
    tensor_in = tensor_in.astype(jnp.float32)
    return (
        tensor_in
        * lax.rsqrt(jnp.mean(tensor_in * tensor_in, axis=-1, keepdims=True) + epsilon)
        * gain_vec
    )


def setup_params(query_logits, forget_logits, input_logits, slack, sudden_decay):
    sequence_total, sequence_span, local_heads = sudden_decay.shape

    def heads_first(tensor):
        return (
            tensor.astype(jnp.float32)
            .reshape(sequence_total, sequence_span, local_heads, -1)
            .transpose(0, 2, 1, 3)
        )

    query_rows = heads_first(query_logits) * KEY ** (-0.5)
    incoming_weights = slack.reshape(local_heads, -1)[None, :, None, :] * jax.nn.sigmoid(
        -heads_first(forget_logits)
    )
    forget_logarithm = jnp.log1p(-incoming_weights) + sudden_decay.transpose(0, 2, 1)[:, :, :, None]
    return (query_rows, incoming_weights, heads_first(input_logits), forget_logarithm)


def block_pass(query_rows, incoming_weights, value_rows, forget_logarithm, initial):
    sequence_total, local_heads, sequence_span, key_width = query_rows.shape
    blocks_here = sequence_span // BLOCK

    def by_block(tensor):
        return tensor.reshape(
            sequence_total, local_heads, blocks_here, BLOCK, tensor.shape[3]
        ).transpose(2, 0, 1, 3, 4)

    causal = jnp.tril(jnp.ones((BLOCK, BLOCK), dtype=bool))

    def advance(carried, portions):
        query_blk, weight_blk, value_blk, forget_blk = portions
        running = jnp.cumsum(forget_blk, axis=2)
        lifted_q = query_blk * jnp.exp(running)
        lifted_k = weight_blk * jnp.exp(-running)
        scores = jnp.einsum("shtk,shuk->shtu", lifted_q, lifted_k, precision=precise)
        scores = jnp.where(causal, scores, 0.0)
        produced = jnp.einsum("shtu,shuv->shtv", scores, value_blk, precision=precise) + jnp.einsum(
            "shtk,shkv->shtv", lifted_q, carried, precision=precise
        )
        ending = running[:, :, -1:, :]
        carried = jnp.exp(ending[:, :, 0, :])[..., None] * carried + jnp.einsum(
            "shuk,shuv->shkv", weight_blk * jnp.exp(ending - running), value_blk, precision=precise
        )
        return (carried, produced)

    final_state, produced = lax.scan(
        advance,
        initial,
        (
            by_block(query_rows),
            by_block(incoming_weights),
            by_block(value_rows),
            by_block(forget_logarithm),
        ),
    )
    return (
        final_state,
        produced.transpose(1, 2, 0, 3, 4).reshape(
            sequence_total, local_heads, sequence_span, value_rows.shape[3]
        ),
    )


def gate_heads(produced, gate_raw, head_norm_gain):
    sequence_total, local_heads, sequence_span, val_width = produced.shape
    mean_sq = jnp.mean(produced * produced, axis=3, keepdims=True)
    scaled = produced * lax.rsqrt(mean_sq + epsilon) * head_norm_gain
    scaled = scaled.transpose(0, 2, 1, 3).reshape(
        sequence_total, sequence_span, local_heads * val_width
    )
    return (scaled * jax.nn.silu(gate_raw.astype(jnp.float32))).astype(jnp.bfloat16)


def join_states(earlier, later):
    earlier_decay, earlier_state = earlier
    later_decay, later_state = later
    return (
        earlier_decay + later_decay,
        jnp.exp(later_decay)[..., None] * earlier_state + later_state,
    )


def recurrence(query_rows, incoming_weights, value_rows, forget_logarithm):
    sequence_total, local_heads, sequence_span, key_width = query_rows.shape
    val_width = value_rows.shape[3]
    through = jnp.cumsum(forget_logarithm, axis=2)
    totals = through[:, :, -1, :]
    head_spans = (0, local_heads)
    head_from, head_upto = head_spans
    zero_state = jnp.zeros(
        (sequence_total, head_upto - head_from, key_width, val_width), jnp.float32
    )
    final_state, produced = block_pass(
        query_rows, incoming_weights, value_rows, forget_logarithm, zero_state
    )
    identity = (jnp.zeros_like(totals), jnp.zeros_like(final_state))
    incoming = entering((totals, final_state), "sp", join_states, identity)
    incoming = incoming[1]
    readout = jnp.einsum(
        "shtk,shkv->shtv", query_rows * jnp.exp(through), incoming, precision=precise
    )
    outputs = produced + readout
    return outputs


def shards(
    tokens,
    input_norm_gain,
    query_weight,
    forget_weight,
    input_weight,
    gate_weight,
    slack,
    sudden_decay,
    head_norm_gain,
    output_weight,
    output_norm_gain,
):
    normed = normalize(tokens, input_norm_gain).astype(jnp.bfloat16)
    matrices = (query_weight, forget_weight, input_weight, gate_weight)
    portion = lax.all_gather(normed, "tp", axis=1, tiled=True)
    joined = lax.optimization_barrier(
        jnp.concatenate(
            [
                jnp.einsum(
                    "std,dc->stc", portion, matrix, preferred_element_type=jnp.float32
                ).astype(jnp.bfloat16)
                for matrix in matrices
            ],
            axis=2,
        )
    )
    query_cols = query_weight.shape[1]
    input_cols = input_weight.shape[1]
    query_logits = joined[:, :, :query_cols]
    forget_logits = joined[:, :, query_cols : 2 * query_cols]
    input_logits = joined[:, :, 2 * query_cols : 2 * query_cols + input_cols]
    gate_raw = joined[:, :, 2 * query_cols + input_cols :]
    query_rows, incoming_weights, value_rows, forget_logarithm = setup_params(
        query_logits, forget_logits, input_logits, slack, sudden_decay
    )
    produced = recurrence(query_rows, incoming_weights, value_rows, forget_logarithm)
    gated_out = gate_heads(produced, gate_raw, head_norm_gain)
    projected = jnp.einsum(
        "stc,cd->std",
        lax.all_gather(gated_out, "tp", axis=2, tiled=True),
        output_weight,
        preferred_element_type=jnp.float32,
    )
    squares = lax.psum(jnp.sum(projected * projected, axis=2, keepdims=True), "tp")
    return (projected * lax.rsqrt(squares / D + epsilon) * output_norm_gain).astype(jnp.bfloat16)


def solution(mesh):
    placed = (
        P(None, ("sp", "tp"), None),
        P(),
        P(None, "tp"),
        P(None, "tp"),
        P(None, "tp"),
        P(None, "tp"),
        P("tp"),
        P(None, "sp", "tp"),
        P(),
        P(None, "tp"),
        P("tp"),
    )
    return jax.shard_map(
        shards, mesh=mesh, in_specs=placed, out_specs=P(None, "sp", "tp"), check_vma=False
    )
```

profile of v0, /device:TPU:0, one launch (start us, length us, event | category | flops | bytes accessed | tf_op | source)
XLA Modules:
  0.0 237.6 jit_solution(12733148455241337241)
XLA Ops:
  6.5 1.7 fusion.26
  8.2 2.5 %fusion.28 = bf16[1,256,2048]{2,1,0:T(8,128)(2,1)} fusion(bf16[1,256,2048]{2,1,0:T(8,128)(2,1)} %param.15, f32[2048]{0:T(1024)} %param.16, f32[256]{0:T(256)S(1)} %add_rsqrt_fusion.2), kind=kLoop, calls=%fused_computation.40 | loop fusion | flops 2097152 | bytes 2106368 | tf_op jit(solution)/shard_map/convert_element_type | solution.py:153
  10.8 35.9 %all-gather.6.cloned.1.call-done = bf16[1,512,2048]{2,1,0:T(8,128)(2,1)} async-done(((bf16[1,256,2048]{2,1,0:T(8,128)(2,1)}), bf16[1,512,2048]{2,1,0:T(8,128)(2,1)}) %all-gather.6.cloned.1.call-update) | async-done | bytes 2097168 | tf_op jit(solution)/shard_map/all_gather | solution.py:155
  46.7 3.7 %fusion.49 = bf16[1,512,512]{1,2,0:T(8,128)(2,1)S(1)} fusion(bf16[2048,512]{1,0:T(8,128)(2,1)} %param.20, bf16[1,512,2048]{2,1,0:T(8,128)(2,1)} %all-gather.6.cloned.1.call-done), kind=kOutput, calls=%fused_computation.59 | convolution fusion | flops 1074003968 | bytes 4718592 | tf_op jit(solution)/shard_map/std,dc->stc/dot_general | solution.py:159
  58.0 3.1 %bitcast_add_fusion.2 = (f32[1,4,128,512]{2,3,1,0:T(8,128)}, f32[1,512,4,128]{3,1,2,0:T(8,128)}) fusion(f32[4,512]{1,0:T(4,128)S(1)} %bitcast.243, f32[1,512,4,128]{3,1,2,0:T(8,128)} %copy.32, f32[4,128]{1,0:T(4,128)S(1)} %bitcast.248), kind=kLoop, calls=%fused_computation.72 | loop fusion | flops 786432 | bytes 3155968 | tf_op jit(solution)/shard_map/add | solution.py:49
  61.1 2.6 %fusion.70 = f32[1,4,512,128]{3,2,1,0:T(8,128)} fusion(f32[1,512,4,128]{3,1,2,0:T(8,128)} %get-tuple-element.175, f32[4,512]{1,0:T(4,128)S(1)} %bitcast.244), kind=kLoop, calls=%fused_computation.76 | loop fusion | flops 524288 | bytes 2105344 | tf_op jit(solution)/shard_map/add | solution.py:49
  64.9 2.6 %copy.34 = f32[1,512,4,128]{3,1,2,0:T(8,128)} copy(f32[1,512,4,128]{1,3,2,0:T(8,128)} %bitcast.233) | data formatting | bytes 2097152 | tf_op jit(solution)/shard_map/mul | solution.py:45
  67.4 57.5 %while.26 = (s32[]{:T(128)}, f32[1,4,128,128]{3,2,1,0:T(8,128)S(1)}, f32[8,1,4,64,128]{4,3,0,2,1:T(8,128)}, f32[8,1,4,64,128]{4,3,0,2,1:T(8,128)}, f32[8,1,4,64,...) while((s32[]{:T(128)}, ...), condition=%wide.region_3.4_spmd.clone, body=%wide.region_1.3_spmd.clone.sunk | while | flops 153571328 | bytes 3174530 | solution.py:80
  71.0 1.9 fusion.96
  73.0 1.6 fusion.94
  78.2 1.9 fusion.96
  80.2 1.6 fusion.94
  85.4 1.9 fusion.96
  87.4 1.6 fusion.94
  92.6 1.9 fusion.96
  94.6 1.6 fusion.94
  99.8 1.9 fusion.96
  101.8 1.6 fusion.94
  107.0 1.9 fusion.96
  109.0 1.6 fusion.94
  114.2 1.9 fusion.96
  116.2 1.6 fusion.94
  121.4 1.9 fusion.96
  123.3 1.6 fusion.94
  125.8 2.5 %copy.46 = f32[4,512,128]{1,2,0:T(8,128)} copy(f32[4,512,128]{2,1,0:T(8,128)} %bitcast.238) | data formatting | bytes 2097152 | tf_op jit(solution)/shard_map/reshape | solution.py:92
  130.3 21.6 %all-gather = f32[16,4,1,128]{3,1,2,0:T(4,128)S(1)} all-gather(f32[1,4,1,128]{3,1,2,0:T(4,128)S(1)} %bitcast.246), channel_id=2, replica_groups=mesh['sp'=16,'tp'=2] {'sp'}, dimensions={0}, use_global_device_ids=true | all-gather | bytes 34816 | tf_op jit(solution)/shard_map/all_gather | solution.py:15
  151.8 24.5 %all-gather.10.cloned.1.call-done = f32[16,4,128,128]{3,2,1,0:T(8,128)} async-done(((f32[1,4,128,128]{3,2,1,0:T(8,128)}), f32[16,4,128,128]{3,2,1,0:T(8,128)}) %all-gather.10.cloned.1.call-update) | async-done | bytes 4194320 | tf_op jit(solution)/shard_map/all_gather | solution.py:15
  177.6 2.9 %multiply_reduce_fusion.1 = (f32[4,512]{1,0:T(4,128)S(1)}, f32[4,512,128]{1,2,0:T(8,128)S(1)}) fusion(f32[4,512,128]{1,2,0:T(8,128)} %copy.46, f32[1,4,128,128]{3,2,1,0:T(8,128)S(1)} %get-tuple-element.94, f32[1,512,4,128]{3,1,2,0:T(8,128)S(1)} %bitcast.229, f32[1,4,128,512]{2,3,1,0:T(8,128)} %copy-done.5), kind=kOutput, calls=%fused_computation.80 | convolution fusion | flops 403699712 | bytes 4464640 | tf_op jit(solution)/shard_map/shtk,shkv->shtv/dot_general | solution.py:133
  183.2 36.3 %all-gather.8.cloned.1.call-done = bf16[1,512,1024]{1,2,0:T(8,128)(2,1)} async-done(((bf16[1,512,512]{1,2,0:T(8,128)(2,1)}), bf16[1,512,1024]{1,2,0:T(8,128)(2,1)}) %all-gather.8.cloned.1.call-update) | async-done | bytes 1048592 | tf_op jit(solution)/shard_map/all_gather | solution.py:180
  219.5 3.8 %multiply_reduce_fusion = (f32[512]{0:T(512)S(1)}, f32[512,1024]{1,0:T(8,128)}) fusion(bf16[1024,1024]{1,0:T(8,128)(2,1)S(1)} %copy-done, bf16[1,512,1024]{1,2,0:T(8,128)(2,1)} %all-gather.8.cloned.1.call-done), kind=kOutput, calls=%fused_computation.51 | convolution fusion | flops 1074789888 | bytes 5244928 | tf_op jit(solution)/shard_map/stc,cd->std/dot_general | solution.py:178
  223.3 4.9 %psum.7 = f32[1,512,1]{1,2,0:T(1,128)S(1)} all-reduce(f32[1,512,1]{1,2,0:T(1,128)S(1)} %bitcast.245), channel_id=1, replica_groups=mesh['sp'=16,'tp'=2] {'tp'}, use_global_device_ids=true, to_apply=%region_10.11 | all-reduce | flops 512 | bytes 4096 | tf_op jit(solution)/shard_map/psum | solution.py:184
  228.2 2.8 %fusion.65 = bf16[1,512,1024]{2,1,0:T(8,128)(2,1)} fusion(f32[512,1024]{1,0:T(8,128)} %get-tuple-element.181, f32[1024]{0:T(1024)S(1)} %copy-done.8, f32[512]{0:T(512)S(1)} %bitcast.247), kind=kLoop, calls=%fused_computation.67 | loop fusion | flops 1572864 | bytes 3151872 | tf_op jit(solution)/shard_map/convert_element_type | solution.py:185
  (117 shorter events, 44.1 us)
Async XLA Ops:
  6.5 212.9 %copy-start = (bf16[1024,1024]{1,0:T(8,128)(2,1)S(1)}, bf16[1024,1024]{1,0:T(8,128)(2,1)}, u32[]{:S(2)}) copy-start(bf16[1024,1024]{1,0:T(8,128)(2,1)} %param.24) | copy-start | bytes 6291460
  6.5 40.2 %all-gather.6.cloned.1.call-start = ((), (), s32[]{:S(2)}) async-start(), calls=%async_computation | async-start | bytes 3145728 | tf_op jit(solution)/shard_map/all_gather | solution.py:155
  10.7 165.6 %all-gather.10.cloned.1.call-start = ((), (), s32[]{:S(2)}) async-start(), calls=%async_computation.2 | async-start | bytes 4456448 | tf_op jit(solution)/shard_map/all_gather | solution.py:15
  46.7 3.7 %copy-start.11 = (bf16[2048,512]{1,0:T(8,128)(2,1)S(1)}, bf16[2048,512]{1,0:T(8,128)(2,1)}, u32[]{:S(2)}) copy-start(bf16[2048,512]{1,0:T(8,128)(2,1)} %param.19) | copy-start | bytes 6291460
  46.7 3.7 %copy-start.14 = (bf16[1,512,2048]{2,1,0:T(8,128)(2,1)S(1)}, bf16[1,512,2048]{2,1,0:T(8,128)(2,1)}, u32[]{:S(2)}) copy-start(bf16[1,512,2048]{2,1,0:T(8,128)(2,1)} %all-gather.6.cloned.1.call-done) | copy-start | bytes 6291460
  50.4 1.6 copy-start.12
  52.0 1.6 copy-start.13
  55.0 1.7 copy-start.3
  56.5 1.6 copy-start.7
  56.5 1.6 copy-start.9
  58.0 5.6 %slice-start = ((bf16[1,512,2048]{1,2,0:T(8,128)(2,1)}), bf16[1,512,512]{1,2,0:T(8,128)(2,1)S(1)}, s32[]{:S(2)}) async-start(bf16[1,512,2048]{1,2,0:T(8,128)(2,1)} %copy-done.3), calls=%async_computation.3 | async-start | bytes 1048576 | tf_op jit(solution)/shard_map/slice | solution.py:171
  125.0 0.7 copy-start.1
  125.0 3.3 %copy-start.6 = (f32[1,4,128,512]{2,3,1,0:T(8,128)S(1)}, f32[1,4,128,512]{2,3,1,0:T(8,128)}, u32[]{:S(2)}) copy-start(f32[1,4,128,512]{2,3,1,0:T(8,128)} %get-tuple-element.174) | copy-start | bytes 3145732
  125.7 93.7 %all-gather.8.cloned.1.call-start = ((), (), s32[]{:S(2)}) async-start(), calls=%async_computation.1 | async-start | bytes 1572864 | tf_op jit(solution)/shard_map/all_gather | solution.py:180
  129.2 1.0 copy-start.5
  176.3 1.2 copy-start.2
  177.6 2.9 %copy-start.10 = (f32[128]{0:T(128)S(1)}, f32[128]{0:T(128)}, u32[]{:S(2)}) copy-start(f32[128]{0:T(128)} %param.23) | copy-start | bytes 1540
  180.4 1.6 copy-start.4
  183.2 45.1 %copy-start.8 = (f32[1024]{0:T(1024)S(1)}, f32[1024]{0:T(1024)}, u32[]{:S(2)}) copy-start(f32[1024]{0:T(1024)} %param.25) | copy-start | bytes 12292
Sparse Core Ops, SparseCore 0:
  10.9 35.8 all-gather.5
  125.8 50.4 all-gather.9
  183.3 36.1 all-gather.7
where the time goes:
time: 239 us; the launch traced here: 238 us
  waiting for transfers between devices  96.8 us (41%)
  matrix products  62.7 us (26%)
  blocking collectives  26.5 us (11%)
  local copies, waits for them, and re-layouts  20.1 us (8%)
  other arithmetic  17.5 us (7%)
  between operations  13.3 us (6%)
    all_gather x1, waiting for transfers between devices, shards(): lax.all_gather(gated_out, 'tp', axis=2, tiled=True)  36.3 us
    all_gather x1, waiting for transfers between devices, shards(): portion = lax.all_gather(normed, 'tp', axis=1, tiled=True)  35.9 us
    all_gather x1, waiting for transfers between devices, entering(): gathered = jax.tree.map(lambda a: lax.all_gather(a, axis), part)  24.5 us
    all_gather x1, blocking collectives, entering(): gathered = jax.tree.map(lambda a: lax.all_gather(a, axis), part)  21.6 us
    dot_general x8, matrix products, advance(): jnp.einsum('shtk,shkv->shtv', lifted_q, carried, precision=precise)  15.5 us
    dot_general x8, matrix products, advance(): jnp.einsum('shuk,shuv->shkv', weight_blk * jnp.exp(ending - running), val...  13 us
    dot_general x8, matrix products, advance(): jnp.einsum('shtk,shuk->shtu', lifted_q, lifted_k, precision=precise)  10.6 us
    dot_general x8, matrix products, advance(): jnp.einsum('shtu,shuv->shtv', scores, value_blk, precision=precise)  9.35 us
  transfers between devices with their start and end apart: 3, of which 3 were waited for; matrix products, arithmetic and copies ran while one was open for 1% of the time, Pallas kernels for 0%

commit v1 on v0

--- a/solution.py
+++ b/solution.py
@@ -8,6 +8,18 @@
 BLOCK = 64
 epsilon = 1e-06
 precise = lax.Precision.HIGHEST
+
+
+def ring_product(x, axis, dim, contribution):
+    length, index = (lax.axis_size(axis), lax.axis_index(axis))
+    left = [(i, (i - 1) % length) for i in range(length)]
+    rows = x.shape[dim]
+    block = x
+    total = contribution(block, index * rows)
+    for step in range(1, length):
+        block = lax.ppermute(block, axis, left)
+        total = total + contribution(block, (index + step) % length * rows)
+    return total
 
 
 def entering(part, axis, combine, identity):
@@ -175,11 +187,16 @@
     )
     produced = recurrence(query_rows, incoming_weights, value_rows, forget_logarithm)
     gated_out = gate_heads(produced, gate_raw, head_norm_gain)
-    projected = jnp.einsum(
-        "stc,cd->std",
-        lax.all_gather(gated_out, "tp", axis=2, tiled=True),
-        output_weight,
-        preferred_element_type=jnp.float32,
+    projected = ring_product(
+        gated_out,
+        "tp",
+        2,
+        lambda part_2, at: jnp.einsum(
+            "stc,cd->std",
+            part_2,
+            lax.dynamic_slice_in_dim(output_weight, at, part_2.shape[2], axis=0),
+            preferred_element_type=jnp.float32,
+        ),
     )
     squares = lax.psum(jnp.sum(projected * projected, axis=2, keepdims=True), "tp")
     return (projected * lax.rsqrt(squares / D + epsilon) * output_norm_gain).astype(jnp.bfloat16)

time: 239 us -> 226 us (0.946)
  the two profiles are of different devices: /device:TPU:0 before, /device:TPU:28 now
where the time goes in v1:
time: 226 us; the launch traced here: 225 us
  waiting for transfers between devices  73.4 us (32%)
  matrix products  61.7 us (27%)
  other arithmetic  32.3 us (14%)
  blocking collectives  21.7 us (10%)
  local copies, waits for them, and re-layouts  19.3 us (9%)
  between operations  13.7 us (6%)
    all_gather x1, waiting for transfers between devices, shards(): portion = lax.all_gather(normed, 'tp', axis=1, tiled=True)  34.1 us
    all_gather x1, waiting for transfers between devices, entering(): gathered = jax.tree.map(lambda a: lax.all_gather(a, axis), part)  27.1 us
    all_gather x1, blocking collectives, entering(): gathered = jax.tree.map(lambda a: lax.all_gather(a, axis), part)  16.7 us
    add x14, other arithmetic, join_states(): jnp.exp(later_decay)[..., None] * earlier_state + later_state  15.7 us
    dot_general x8, matrix products, advance(): jnp.einsum('shtk,shkv->shtv', lifted_q, carried, precision=precise)  15.5 us
    dot_general x8, matrix products, advance(): jnp.einsum('shuk,shuv->shkv', weight_blk * jnp.exp(ending - running), val...  13 us
    ppermute x1, waiting for transfers between devices, ring_product(): block = lax.ppermute(block, axis, left)  12.2 us
    dot_general x8, matrix products, advance(): jnp.einsum('shtk,shuk->shtu', lifted_q, lifted_k, precision=precise)  10.6 us
  transfers between devices with their start and end apart: 3, of which 3 were waited for; matrix products, arithmetic and copies ran while one was open for 2% of the time, Pallas kernels for 0%

profile of v1, /device:TPU:28, one launch (start us, length us, event | category | flops | bytes accessed | tf_op | source)
XLA Modules:
  0.0 224.7 jit_solution(2842859089587822508)
XLA Ops:
  6.5 1.7 fusion.26
  8.2 2.5 %fusion.28 = bf16[1,256,2048]{2,1,0:T(8,128)(2,1)} fusion(bf16[1,256,2048]{2,1,0:T(8,128)(2,1)} %param.15, f32[2048]{0:T(1024)} %param.16, f32[256]{0:T(256)S(1)} %add_rsqrt_fusion.2), kind=kLoop, calls=%fused_computation.40 | loop fusion | flops 2097152 | bytes 2106368 | tf_op jit(solution)/shard_map/convert_element_type | solution.py:165
  10.8 34.1 %all-gather.5.cloned.1.call-done = bf16[1,512,2048]{2,1,0:T(8,128)(2,1)} async-done(((bf16[1,256,2048]{2,1,0:T(8,128)(2,1)}), bf16[1,512,2048]{2,1,0:T(8,128)(2,1)}) %all-gather.5.cloned.1.call-update) | async-done | bytes 2097168 | tf_op jit(solution)/shard_map/all_gather | solution.py:167
  44.9 3.7 %fusion.49 = bf16[1,512,512]{1,2,0:T(8,128)(2,1)S(1)} fusion(bf16[2048,512]{1,0:T(8,128)(2,1)} %param.20, bf16[1,512,2048]{2,1,0:T(8,128)(2,1)} %all-gather.5.cloned.1.call-done), kind=kOutput, calls=%fused_computation.60 | convolution fusion | flops 1074003968 | bytes 4718592 | tf_op jit(solution)/shard_map/std,dc->stc/dot_general | solution.py:171
  56.2 3.1 %bitcast_add_fusion.2 = (f32[1,4,128,512]{2,3,1,0:T(8,128)}, f32[1,512,4,128]{3,1,2,0:T(8,128)}) fusion(f32[4,512]{1,0:T(4,128)S(1)} %bitcast.245, f32[1,512,4,128]{3,1,2,0:T(8,128)} %copy.32, f32[4,128]{1,0:T(4,128)S(1)} %bitcast.250), kind=kLoop, calls=%fused_computation.71 | loop fusion | flops 786432 | bytes 3155968 | tf_op jit(solution)/shard_map/add | solution.py:61
  59.3 2.6 %fusion.68 = f32[1,4,512,128]{3,2,1,0:T(8,128)} fusion(f32[1,512,4,128]{3,1,2,0:T(8,128)} %get-tuple-element.175, f32[4,512]{1,0:T(4,128)S(1)} %bitcast.246), kind=kLoop, calls=%fused_computation.75 | loop fusion | flops 524288 | bytes 2105344 | tf_op jit(solution)/shard_map/add | solution.py:61
  63.1 2.5 %copy.34 = f32[1,512,4,128]{3,1,2,0:T(8,128)} copy(f32[1,512,4,128]{1,3,2,0:T(8,128)} %bitcast.235) | data formatting | bytes 2097152 | tf_op jit(solution)/shard_map/mul | solution.py:57
  65.6 57.5 %while.26 = (s32[]{:T(128)}, f32[1,4,128,128]{3,2,1,0:T(8,128)S(1)}, f32[8,1,4,64,128]{4,3,0,2,1:T(8,128)}, f32[8,1,4,64,128]{4,3,0,2,1:T(8,128)}, f32[8,1,4,64,...) while((s32[]{:T(128)}, ...), condition=%wide.region_3.4_spmd.clone, body=%wide.region_1.3_spmd.clone.sunk | while | flops 153571328 | bytes 3174530 | solution.py:92
  69.2 1.9 fusion.100
  71.2 1.6 fusion.98
  76.4 1.9 fusion.100
  78.4 1.6 fusion.98
  83.6 1.9 fusion.100
  85.6 1.6 fusion.98
  90.8 1.9 fusion.100
  92.7 1.6 fusion.98
  98.0 1.9 fusion.100
  99.9 1.6 fusion.98
  105.2 1.9 fusion.100
  112.4 1.9 fusion.100
  114.3 1.6 fusion.98
  119.6 1.9 fusion.100
  121.5 1.6 fusion.98
  123.9 2.5 %copy.46 = f32[4,512,128]{1,2,0:T(8,128)} copy(f32[4,512,128]{2,1,0:T(8,128)} %bitcast.240) | data formatting | bytes 2097152 | tf_op jit(solution)/shard_map/reshape | solution.py:104
  128.4 16.7 %all-gather = f32[16,4,1,128]{3,1,2,0:T(4,128)S(1)} all-gather(f32[1,4,1,128]{3,1,2,0:T(4,128)S(1)} %bitcast.248), channel_id=2, replica_groups=mesh['sp'=16,'tp'=2] {'sp'}, dimensions={0}, use_global_device_ids=true | all-gather | bytes 34816 | tf_op jit(solution)/shard_map/all_gather | solution.py:27
  145.2 27.1 %all-gather.7.cloned.1.call-done = f32[16,4,128,128]{3,2,1,0:T(8,128)} async-done(((f32[1,4,128,128]{3,2,1,0:T(8,128)}), f32[16,4,128,128]{3,2,1,0:T(8,128)}) %all-gather.7.cloned.1.call-update) | async-done | bytes 4194320 | tf_op jit(solution)/shard_map/all_gather | solution.py:27
  172.3 16.5 %while.25 = (s32[]{:T(128)}, f32[1,4,128,128]{3,2,1,0:T(8,128)S(1)}, s32[]{:T(128)}, f32[16,1,4,128]{3,2,1,0:T(4,128)S(1)}, f32[16,1,4,128,128]{4,3,2,1,0:T(8,128)}, /*index=5*/s32[]{:T(128)}, s32[]{:T(128)}, s32[]{:T(128)}) while((s32[]{:T(128)}, f32[1,4,128,128]{3,2,1,0:T(8,128)S(1)}, s32[]{:T(128)}, f32[16,1,4,128]{3,2,1,0:T(4,128)S(1)}, ...), condition=%wide.region_7.8_spmd, body=%wide.region_6.7_spmd.sunk | while | flops 131077 | bytes 792711 | solution.py:35
  188.8 2.9 %multiply_reduce_fusion.1 = (f32[4,512]{1,0:T(4,128)S(1)}, f32[4,512,128]{1,2,0:T(8,128)S(1)}) fusion(f32[4,512,128]{1,2,0:T(8,128)} %copy.46, f32[1,4,128,128]{3,2,1,0:T(8,128)S(1)} %get-tuple-element.94, f32[1,512,4,128]{3,1,2,0:T(8,128)S(1)} %bitcast.231, f32[1,4,128,512]{2,3,1,0:T(8,128)} %copy-done.5), kind=kOutput, calls=%fused_computation.82 | convolution fusion | flops 403699712 | bytes 4464640 | tf_op jit(solution)/shard_map/shtk,shkv->shtv/dot_general | solution.py:145
  195.9 12.2 %collective-permute-done = bf16[1,512,512]{1,2,0:T(8,128)(2,1)S(1)} collective-permute-done((bf16[1,512,512]{1,2,0:T(8,128)(2,1)S(1)}, bf16[1,512,512]{1,2,0:T(8,128)(2,1)S(1)}, u32[]{:S(2)}, u32[]{:S(2)}) %collective-permute-start) | collective-permute-done | bytes 524320 | tf_op jit(solution)/shard_map/ppermute | solution.py:20
  208.0 2.1 multiply_reduce_fusion
  210.1 4.9 %psum.7 = f32[1,512,1]{1,2,0:T(1,128)S(1)} all-reduce(f32[1,512,1]{1,2,0:T(1,128)S(1)} %bitcast.247), channel_id=1, replica_groups=mesh['sp'=16,'tp'=2] {'tp'}, use_global_device_ids=true, to_apply=%region_10.11 | all-reduce | flops 512 | bytes 4096 | tf_op jit(solution)/shard_map/psum | solution.py:201
  215.0 2.8 %fusion.65 = bf16[1,512,1024]{2,1,0:T(8,128)(2,1)} fusion(f32[512,1024]{1,0:T(8,128)} %get-tuple-element.181, f32[1024]{0:T(1024)S(1)} %copy-done.8, f32[512]{0:T(512)S(1)} %bitcast.249), kind=kLoop, calls=%fused_computation.68 | loop fusion | flops 1572864 | bytes 3151872 | tf_op jit(solution)/shard_map/convert_element_type | solution.py:202
  (145 shorter events, 61.8 us)
Async XLA Ops:
  6.5 188.6 %copy-start = (bf16[1024,1024]{1,0:T(8,128)(2,1)S(1)}, bf16[1024,1024]{1,0:T(8,128)(2,1)}, u32[]{:S(2)}) copy-start(bf16[1024,1024]{1,0:T(8,128)(2,1)} %param.24) | copy-start | bytes 6291460
  6.5 38.4 %all-gather.5.cloned.1.call-start = ((), (), s32[]{:S(2)}) async-start(), calls=%async_computation | async-start | bytes 3145728 | tf_op jit(solution)/shard_map/all_gather | solution.py:167
  10.7 161.6 %all-gather.7.cloned.1.call-start = ((), (), s32[]{:S(2)}) async-start(), calls=%async_computation.1 | async-start | bytes 4456448 | tf_op jit(solution)/shard_map/all_gather | solution.py:27
  44.9 3.7 %copy-start.11 = (bf16[2048,512]{1,0:T(8,128)(2,1)S(1)}, bf16[2048,512]{1,0:T(8,128)(2,1)}, u32[]{:S(2)}) copy-start(bf16[2048,512]{1,0:T(8,128)(2,1)} %param.19) | copy-start | bytes 6291460
  44.9 3.7 %copy-start.14 = (bf16[1,512,2048]{2,1,0:T(8,128)(2,1)S(1)}, bf16[1,512,2048]{2,1,0:T(8,128)(2,1)}, u32[]{:S(2)}) copy-start(bf16[1,512,2048]{2,1,0:T(8,128)(2,1)} %all-gather.5.cloned.1.call-done) | copy-start | bytes 6291460
  48.6 1.6 copy-start.12
  50.2 1.6 copy-start.13
  53.2 1.7 copy-start.3
  54.7 1.5 copy-start.7
  54.7 1.5 copy-start.9
  56.2 5.6 %slice-start = ((bf16[1,512,2048]{1,2,0:T(8,128)(2,1)}), bf16[1,512,512]{1,2,0:T(8,128)(2,1)S(1)}, s32[]{:S(2)}) async-start(bf16[1,512,2048]{1,2,0:T(8,128)(2,1)} %copy-done.3), calls=%async_computation.2 | async-start | bytes 1048576 | tf_op jit(solution)/shard_map/slice | solution.py:183
  123.2 0.7 copy-start.1
  123.2 3.3 %copy-start.6 = (f32[1,4,128,512]{2,3,1,0:T(8,128)S(1)}, f32[1,4,128,512]{2,3,1,0:T(8,128)}, u32[]{:S(2)}) copy-start(f32[1,4,128,512]{2,3,1,0:T(8,128)} %get-tuple-element.174) | copy-start | bytes 3145732
  127.4 1.0 copy-start.5
  172.3 16.5 %copy-start.2 = (f32[8,1,4,64,128]{4,3,0,2,1:T(8,128)S(1)}, f32[8,1,4,64,128]{4,3,0,2,1:T(8,128)}, u32[]{:S(2)}) copy-start(f32[8,1,4,64,128]{4,3,0,2,1:T(8,128)} %get-tuple-element.315) | copy-start | bytes 3145732
  188.8 2.9 %copy-start.10 = (f32[128]{0:T(128)S(1)}, f32[128]{0:T(128)}, u32[]{:S(2)}) copy-start(f32[128]{0:T(128)} %param.23) | copy-start | bytes 1540
  191.7 1.6 copy-start.4
  193.6 14.4 %collective-permute-start = (bf16[1,512,512]{1,2,0:T(8,128)(2,1)S(1)}, bf16[1,512,512]{1,2,0:T(8,128)(2,1)S(1)}, u32[]{:S(2)}, u32[]{:S(2)}) collective-permute-start(bf16[1,512,512]{1,2,0:T(8,128)(2,1)S(1)} %fusion.75), channel_id=1, source_target_pairs={{0,1},{1,0},{2,3},{3,2},{4,5},{5,4},{6,7},{7,6},{8,9},{9,8},{10,11... | collective-permute-start | bytes 1572872 | tf_op jit(solution)/shard_map/ppermute | solution.py:20
  195.9 19.2 %copy-start.8 = (f32[1024]{0:T(1024)S(1)}, f32[1024]{0:T(1024)}, u32[]{:S(2)}) copy-start(f32[1024]{0:T(1024)} %param.25) | copy-start | bytes 12292
Sparse Core Ops, SparseCore 0:
  10.9 34.0 all-gather.4
  124.0 48.2 all-gather.6
